TPU v7x, 32 devices: a whole 2x2x4 slice. The times are simulated.
32 devices in a mesh: sp: 8 (over z, x), tp: 4 (over y, core).
Axes of the slice: x: 2, y: 2, z: 4, core: 2. Of those that a mesh axis runs over, the one named last changes fastest.
Arguments:
- latents: bfloat16 [4096, 2048], P(('sp', 'tp')), may hold values from -6 to 6
- context: bfloat16 [512, 2048], P('sp'), may hold values from -6 to 6
- cond: float32 [2048], P('sp'), may hold values from -6 to 6
- ctx_cond: float32 [2048], P('sp'), may hold values from -6 to 6
- mod_weight: float32 [2048, 6144], P('sp', 'tp'), may hold values from -0.125 to 0.125
- query_weight: bfloat16 [2048, 2048], P(None, 'tp'), may hold values from -1 to 1, as said below
- key_matrix: bfloat16 [2048, 1024], P(None, 'tp'), may hold values from -1 to 1, as said below
- value_matrix: bfloat16 [2048, 1024], P(None, 'tp'), may hold values from -0.125 to 0.125
- out_weight: bfloat16 [2048, 2048], P('tp'), may hold values from -0.125 to 0.125
- query_gain: float32 [128], replicated, may hold values from 0.7 to 7
- key_gain: float32 [128], replicated, may hold values from 0.7 to 7
Outputs:
- updated: bfloat16 [4096, 2048], P(('sp', 'tp'))
Inputs may be any that keep to these rules, and one draw needn't show every extreme that they name: `query_weight`: entries of order 2048 to the power -1/2. `key_matrix`: entries of order 2048 to the power -1/2.
All inputs are finite; a program needn't handle non-finite values.
Results may differ from a plain program's by a relative error of at most 0.0085.
The roundings to bfloat16 on the way count: a program that leaves them out, or rounds other values in their place, can miss the bound.
Values may be sent and summed in bfloat16 or wider, within the bound.
A program may use at most 128 MiB of HBM per device.

v0:
```python
import math
import jax
import jax.numpy as jnp
from jax import lax
from jax.sharding import PartitionSpec as P

GRID_W = 64
NORM_EPS = 1e-06
ROPE_BASE = 10000.0


def normalize(latent_value_rows):
    return latent_value_rows * lax.rsqrt(
        jnp.mean(latent_value_rows * latent_value_rows, axis=-1, keepdims=True) + NORM_EPS
    )


def rotate(latent_value_rows, positions):
    quarter = latent_value_rows.shape[-1] // 2
    inv_freq = ROPE_BASE ** (-jnp.arange(quarter, dtype=jnp.float32) / quarter)
    angles = positions.astype(jnp.float32)[:, None] * inv_freq[None, :]
    cos_table = jnp.cos(angles)[:, None, :]
    sin_table = jnp.sin(angles)[:, None, :]
    first, second = (latent_value_rows[..., :quarter], latent_value_rows[..., quarter:])
    return jnp.concatenate(
        [first * cos_table - second * sin_table, second * cos_table + first * sin_table], axis=-1
    )


def axial(latent_value_rows, positions):
    half_dim = latent_value_rows.shape[-1] // 2
    return jnp.concatenate(
        [
            rotate(latent_value_rows[..., :half_dim], positions // GRID_W),
            rotate(latent_value_rows[..., half_dim:], positions % GRID_W),
        ],
        axis=-1,
    )


def modulate(latent_value_rows, mod_row):
    model_width = latent_value_rows.shape[-1]
    shift_vec = mod_row[:model_width]
    scale_vec = mod_row[model_width : 2 * model_width]
    return (
        normalize(latent_value_rows.astype(jnp.float32)) * (1.0 + scale_vec) + shift_vec
    ).astype(jnp.bfloat16)


def body(
    latents,
    context,
    cond,
    ctx_cond,
    mod_weight,
    query_weight,
    key_matrix,
    value_matrix,
    out_weight,
    query_gain,
    key_gain,
):
    model_width = latents.shape[1]
    head_dim = query_gain.shape[0]
    sp_count = lax.axis_size("sp")
    partials = jnp.dot(
        jax.nn.silu(jnp.stack([cond, ctx_cond])), mod_weight, precision=lax.Precision.HIGHEST
    )
    summed = lax.psum(partials, "sp")
    modulation = lax.all_gather(summed, "tp", axis=1, tiled=True)
    gate_vec = modulation[0, 2 * model_width :]
    normalised_rows = modulate(latents, modulation[0])
    prefix_normalised = modulate(context, modulation[1])
    query_cols = query_weight.shape[1]
    key_cols = key_matrix.shape[1]
    piece = lax.all_gather(normalised_rows, "tp", axis=0, tiled=True)
    projected = jnp.concatenate(
        [
            jnp.dot(piece, query_weight, preferred_element_type=jnp.float32),
            jnp.dot(piece, key_matrix, preferred_element_type=jnp.float32),
            jnp.dot(piece, value_matrix, preferred_element_type=jnp.float32),
        ],
        axis=1,
    )
    row_count = projected.shape[0]
    positions = lax.axis_index("sp") * row_count + jnp.arange(row_count, dtype=jnp.int32)
    query_heads = projected[:, :query_cols].reshape(row_count, -1, head_dim)
    query_heads = axial(normalize(query_heads) * query_gain, positions).astype(jnp.bfloat16)
    key_heads = projected[:, query_cols : query_cols + key_cols].reshape(row_count, -1, head_dim)
    key_heads = axial(normalize(key_heads) * key_gain, positions).astype(jnp.bfloat16)
    value_heads = (
        projected[:, query_cols + key_cols :].reshape(row_count, -1, head_dim).astype(jnp.bfloat16)
    )
    key_part = jnp.dot(prefix_normalised, key_matrix, preferred_element_type=jnp.float32).reshape(
        prefix_normalised.shape[0], -1, head_dim
    )
    value_part = jnp.dot(
        prefix_normalised, value_matrix, preferred_element_type=jnp.float32
    ).reshape(prefix_normalised.shape[0], -1, head_dim)
    local_keys = (normalize(key_part) * key_gain).astype(jnp.bfloat16)
    local_values = value_part.astype(jnp.bfloat16)
    prefix_keys, prefix_values = (
        lax.all_gather(local_keys, "sp", axis=0, tiled=True),
        lax.all_gather(local_values, "sp", axis=0, tiled=True),
    )
    kv_local = key_heads.shape[1]
    group_size = query_heads.shape[1] // kv_local
    grouped = query_heads.reshape(row_count, kv_local, group_size, head_dim).transpose(1, 2, 0, 3)
    grouped = grouped.reshape(kv_local, group_size * row_count, head_dim)
    inv_root = head_dim ** (-0.5)
    lift = math.log(sp_count * row_count / (2.0 * prefix_keys.shape[0]))
    ctx_scores = (
        jnp.einsum("hqd,khd->hqk", grouped, prefix_keys, preferred_element_type=jnp.float32)
        * inv_root
        + lift
    )
    top_init = jnp.max(ctx_scores, axis=-1)
    ctx_weights = jnp.exp(ctx_scores - top_init[..., None])
    initial = (
        top_init,
        jnp.sum(ctx_weights, axis=-1),
        jnp.einsum(
            "hqk,khd->hqd",
            ctx_weights.astype(jnp.bfloat16),
            prefix_values,
            preferred_element_type=jnp.float32,
        ),
    )

    def update(state_now, key_block, value_block):
        top_old, total_old, acc_old = state_now
        scores = (
            jnp.einsum("hqd,khd->hqk", grouped, key_block, preferred_element_type=jnp.float32)
            * inv_root
        )
        top_new = jnp.maximum(top_old, jnp.max(scores, axis=-1))
        factor = jnp.exp(top_old - top_new)
        weights_now = jnp.exp(scores - top_new[..., None])
        acc_new = acc_old * factor[..., None] + jnp.einsum(
            "hqk,khd->hqd",
            weights_now.astype(jnp.bfloat16),
            value_block,
            preferred_element_type=jnp.float32,
        )
        return (top_new, total_old * factor + jnp.sum(weights_now, axis=-1), acc_new)

    key_piece = lax.all_gather(key_heads, "sp", axis=0, tiled=True)
    value_piece = lax.all_gather(value_heads, "sp", axis=0, tiled=True)
    key_count = key_piece.shape[0]
    rows_per_block = math.gcd(key_count, 2048)
    block_count = key_count // rows_per_block
    key_blocks = key_piece.reshape(block_count, rows_per_block, kv_local, head_dim)
    value_blocks = value_piece.reshape(block_count, rows_per_block, kv_local, head_dim)

    def one_step(state_in, blocks_in):
        return (update(state_in, blocks_in[0], blocks_in[1]), None)

    state_out, _ = lax.scan(one_step, initial, (key_blocks, value_blocks))
    top_fin, total_fin, acc_fin = state_out
    attended = (acc_fin / total_fin[..., None]).astype(jnp.bfloat16)
    attended = (
        attended.reshape(kv_local, group_size, row_count, head_dim)
        .transpose(2, 0, 1, 3)
        .reshape(row_count, -1)
    )
    mixed_rows = lax.psum_scatter(
        jnp.dot(attended, out_weight, preferred_element_type=jnp.float32).astype(jnp.bfloat16),
        "tp",
        scatter_dimension=0,
        tiled=True,
    ).astype(jnp.float32)
    return (latents.astype(jnp.float32) + gate_vec * normalize(mixed_rows)).astype(jnp.bfloat16)


def solution(mesh):
    placed = (
        P(("sp", "tp"), None),
        P("sp", None),
        P("sp"),
        P("sp"),
        P("sp", "tp"),
        P(None, "tp"),
        P(None, "tp"),
        P(None, "tp"),
        P("tp", None),
        P(),
        P(),
    )
    return jax.shard_map(
        body, mesh=mesh, in_specs=placed, out_specs=P(("sp", "tp"), None), check_vma=False
    )
```

profile of v0, /device:TPU:0, one launch (start us, length us, event | category | flops | bytes accessed | tf_op | source)
XLA Modules:
  0.0 286.1 jit_solution(9915169423210026204)
XLA Ops:
  6.5 2.4 fusion.41
  9.0 38.8 %psum.7 = f32[2,1536]{1,0:T(2,128)S(1)} all-reduce(f32[2,1536]{1,0:T(2,128)S(1)} %fusion.41), channel_id=1, replica_groups=mesh['sp'=8,'tp'=4] {'sp'}, use_global_device_ids=true, to_apply=%region_0.1 | all-reduce | flops 3072 | bytes 24576 | tf_op jit(solution)/shard_map/psum | solution.py:69
  47.8 5.2 %all_gather.18 = f32[2,6144]{1,0:T(2,128)S(1)} all-gather(f32[2,1536]{1,0:T(2,128)S(1)} %psum.7), channel_id=1, replica_groups=mesh['sp'=8,'tp'=4] {'tp'}, dimensions={1}, use_global_device_ids=true | all-gather | bytes 61440 | tf_op jit(solution)/shard_map/all_gather | solution.py:70
  54.9 2.1 fusion.30
  59.6 17.4 %all-gather.4.cloned.1.call-done = bf16[512,2048]{1,0:T(8,128)(2,1)} async-done(((bf16[128,2048]{1,0:T(8,128)(2,1)}), bf16[512,2048]{1,0:T(8,128)(2,1)}) %all-gather.4.cloned.1.call-update) | async-done | bytes 2097168 | tf_op jit(solution)/shard_map/all_gather | solution.py:76
  77.0 4.0 %multiply_reduce_fusion.1 = (f32[512,2]{0,1:T(2,128)}, f32[512,256]{0,1:T(8,128)}) fusion(bf16[512,2048]{1,0:T(8,128)(2,1)} %all-gather.4.cloned.1.call-done, bf16[2048,256]{1,0:T(8,128)(2,1)} %param.19), kind=kOutput, calls=%fused_computation.57 | convolution fusion | flops 537132032 | bytes 3674112 | tf_op jit(solution)/shard_map/dot_general | solution.py:80
  87.3 3.3 %convolution_convert_fusion.1 = bf16[512,256]{0,1:T(8,128)(2,1)} fusion(bf16[512,2048]{1,0:T(8,128)(2,1)} %all-gather.4.cloned.1.call-done, bf16[2048,256]{1,0:T(8,128)(2,1)} %param.20), kind=kOutput, calls=%fused_computation.32 | convolution fusion | flops 537001984 | bytes 3407872 | tf_op jit(solution)/shard_map/dot_general | solution.py:81
  98.4 31.6 %all_gather.20 = bf16[512,2,128]{2,0,1:T(8,128)(2,1)S(1)} all-gather(bf16[64,2,128]{2,0,1:T(8,128)(2,1)S(1)} %fusion.37), channel_id=1, replica_groups=mesh['sp'=8,'tp'=4] {'sp'}, dimensions={0}, use_global_device_ids=true | all-gather | bytes 294912 | tf_op jit(solution)/shard_map/all_gather | solution.py:103
  129.9 33.5 %all_gather.21 = bf16[512,2,128]{2,0,1:T(8,128)(2,1)} all-gather(bf16[64,2,128]{2,0,1:T(8,128)(2,1)S(1)} %bitcast.103), channel_id=1, replica_groups=mesh['sp'=8,'tp'=4] {'sp'}, dimensions={0}, use_global_device_ids=true | all-gather | bytes 294912 | tf_op jit(solution)/shard_map/all_gather | solution.py:104
  163.5 3.6 %multiply_reduce_fusion = (f32[512,4]{0,1:T(4,128)S(1)}, f32[512,512]{0,1:T(8,128)S(1)}) fusion(bf16[512,2048]{1,0:T(8,128)(2,1)} %all-gather.4.cloned.1.call-done, bf16[2048,512]{1,0:T(8,128)(2,1)} %param.18), kind=kOutput, calls=%fused_computation.44 | convolution fusion | flops 1074264064 | bytes 5251072 | tf_op jit(solution)/shard_map/dot_general | solution.py:79
  169.6 1.9 copy.74
  171.5 1.9 copy.75
  173.5 1.9 pad_maximum_fusion
  179.0 10.1 %all-gather.8.cloned.1.call-done = bf16[4096,2,128]{2,0,1:T(8,128)(2,1)} async-done(((bf16[512,2,128]{2,0,1:T(8,128)(2,1)}), bf16[4096,2,128]{2,0,1:T(8,128)(2,1)}) %all-gather.8.cloned.1.call-update) | async-done | bytes 2097168 | tf_op jit(solution)/shard_map/all_gather | solution.py:148
  189.1 52.1 %while.14 = (s32[]{:T(128)}, f32[2,1024]{1,0:T(2,128)S(1)}, f32[2,1024]{1,0:T(2,128)S(1)}, f32[2,1024,128]{2,1,0:T(8,128)S(1)}, bf16[2,2048,2,128]{3,1,0,2:T(8,1...) while((s32[]{:T(128)}, f32[2,1024]{1,0:T(2,128)S(1)}, ...), condition=%wide.region_11.12_spmd, body=%wide.region_8.11_spmd.sunk | while | flops 2181566464 | bytes 55182420 | solution.py:158
  189.1 9.4 %bitcast_reduce_fusion.2 = (f32[2,1024]{1,0:T(2,128)S(1)}, f32[2,2048,1024]{2,1,0:T(8,128)}) fusion(bf16[2,1024,128]{2,1,0:T(8,128)(2,1)} %get-tuple-element.194, bf16[2,2048,2,128]{3,1,0,2:T(8,128)(2,1)} %get-tuple-element.193, s32[]{:T(128)} %get-tuple-element.181), kind=kOutput, calls=%fused_computation.1.clone.1 | convolution fusion | flops 1082128384 | bytes 18358784 | tf_op jit(solution)/shard_map/while/body/eval_jaxpr/hqd,khd->hqk/dot_general | solution.py:133
  198.5 8.5 %fusion.80 = f32[2,1024]{1,0:T(2,128)S(1)} fusion(f32[2,2048,1024]{2,1,0:T(8,128)} %get-tuple-element.170, f32[2,1024]{1,0:T(2,128)S(1)} %max.4), kind=kLoop, calls=%fused_computation.4.clone.1 | loop fusion | flops 12580864 | bytes 16793600 | tf_op jit(solution)/shard_map/while/body/eval_jaxpr/reduce_sum | solution.py:145
  207.0 8.1 %fusion.81 = f32[2,1024,128]{2,1,0:T(8,128)S(1)} fusion(f32[2,2048,1024]{2,1,0:T(8,128)} %get-tuple-element.170, f32[2,1024]{1,0:T(2,128)S(1)} %max.4, bf16[2,2048,2,128]{3,1,0,2:T(8,128)(2,1)} %get-tuple-element.195, s32[]{:T(128)} %get-tuple-element.181, f32[2,1024,128]{2,1,0:T(8,128)S(1)} %get-tuple-element.184, f32[2,1024]{1,0:T(2,128)S(1)} %get-tuple-element.172), kind=kOutput, calls=%fused_computation.6.clone.1 | convolution fusion | flops 1086849024 | bytes 19939840 | tf_op jit(solution)/shard_map/while/body/eval_jaxpr/hqk,khd->hqd/dot_general | solution.py:139
  215.1 9.4 %bitcast_reduce_fusion.2 = (f32[2,1024]{1,0:T(2,128)S(1)}, f32[2,2048,1024]{2,1,0:T(8,128)}) fusion(bf16[2,1024,128]{2,1,0:T(8,128)(2,1)} %get-tuple-element.194, bf16[2,2048,2,128]{3,1,0,2:T(8,128)(2,1)} %get-tuple-element.193, s32[]{:T(128)} %get-tuple-element.181), kind=kOutput, calls=%fused_computation.1.clone.1 | convolution fusion | flops 1082128384 | bytes 18358784 | tf_op jit(solution)/shard_map/while/body/eval_jaxpr/hqd,khd->hqk/dot_general | solution.py:133
  224.5 8.5 %fusion.80 = f32[2,1024]{1,0:T(2,128)S(1)} fusion(f32[2,2048,1024]{2,1,0:T(8,128)} %get-tuple-element.170, f32[2,1024]{1,0:T(2,128)S(1)} %max.4), kind=kLoop, calls=%fused_computation.4.clone.1 | loop fusion | flops 12580864 | bytes 16793600 | tf_op jit(solution)/shard_map/while/body/eval_jaxpr/reduce_sum | solution.py:145
  233.1 8.1 %fusion.81 = f32[2,1024,128]{2,1,0:T(8,128)S(1)} fusion(f32[2,2048,1024]{2,1,0:T(8,128)} %get-tuple-element.170, f32[2,1024]{1,0:T(2,128)S(1)} %max.4, bf16[2,2048,2,128]{3,1,0,2:T(8,128)(2,1)} %get-tuple-element.195, s32[]{:T(128)} %get-tuple-element.181, f32[2,1024,128]{2,1,0:T(8,128)S(1)} %get-tuple-element.184, f32[2,1024]{1,0:T(2,128)S(1)} %get-tuple-element.172), kind=kOutput, calls=%fused_computation.6.clone.1 | convolution fusion | flops 1086849024 | bytes 19939840 | tf_op jit(solution)/shard_map/while/body/eval_jaxpr/hqk,khd->hqd/dot_general | solution.py:139
  243.6 2.6 convolution_convert_fusion
  246.3 29.9 %reduce-scatter.2.cloned.1.call-done = bf16[128,2048]{1,0:T(8,128)(2,1)} async-done(((bf16[512,2048]{1,0:T(8,128)(2,1)}), bf16[128,2048]{1,0:T(8,128)(2,1)}) %reduce-scatter.2.cloned.1.call-update) | async-done | bytes 524304 | tf_op jit(solution)/shard_map/reduce_scatter | solution.py:166
  277.4 2.1 fusion.31
  (79 shorter events, 28.3 us)
Async XLA Ops:
  6.5 237.1 %copy-start = (bf16[512,2048]{1,0:T(8,128)(2,1)S(1)}, bf16[512,2048]{1,0:T(8,128)(2,1)}, u32[]{:S(2)}) copy-start(bf16[512,2048]{1,0:T(8,128)(2,1)} %param.21) | copy-start | bytes 6291460
  6.5 70.5 %all-gather.4.cloned.1.call-start = ((), (), s32[]{:S(2)}) async-start(), calls=%async_computation.1 | async-start | bytes 2621440 | tf_op jit(solution)/shard_map/all_gather | solution.py:76
  57.0 122.0 %all-gather.6.cloned.1.call-start = ((), (), s32[]{:S(2)}) async-start(), calls=%async_computation.2 | async-start | bytes 2359296 | tf_op jit(solution)/shard_map/all_gather | solution.py:147
  57.6 19.4 %copy-start.6 = (f32[512,32]{0,1:T(8,128)}, f32[512,32]{0,1:T(8,128)S(1)}, u32[]{:S(2)}) copy-start(f32[512,32]{0,1:T(8,128)S(1)} %get-tuple-element.112) | copy-start | bytes 196612
  57.6 19.4 %copy-start.8 = (f32[512,32]{0,1:T(8,128)}, f32[512,32]{0,1:T(8,128)S(1)}, u32[]{:S(2)}) copy-start(f32[512,32]{0,1:T(8,128)S(1)} %get-tuple-element.113) | copy-start | bytes 196612
  81.0 5.5 %copy-start.3 = (bf16[64,2048]{1,0:T(8,128)(2,1)S(1)}, bf16[64,2048]{1,0:T(8,128)(2,1)}, u32[]{:S(2)}) copy-start(bf16[64,2048]{1,0:T(8,128)(2,1)} %param.14) | copy-start | bytes 786436
  85.3 8.4 %copy-start.4 = (bf16[2048,256]{1,0:T(8,128)(2,1)S(1)}, bf16[2048,256]{1,0:T(8,128)(2,1)}, u32[]{:S(2)}) copy-start(bf16[2048,256]{1,0:T(8,128)(2,1)} %param.19) | copy-start | bytes 3145732
  86.5 102.6 %all-gather.8.cloned.1.call-start = ((), (), s32[]{:S(2)}) async-start(), calls=%async_computation.3 | async-start | bytes 2359296 | tf_op jit(solution)/shard_map/all_gather | solution.py:148
  92.4 183.8 %reduce-scatter.2.cloned.1.call-start = ((), (), s32[]{:S(2)}) async-start(), calls=%async_computation.4 | async-start | bytes 2621440 | tf_op jit(solution)/shard_map/reduce_scatter | solution.py:166
  93.1 0.6 copy-start.11
  163.4 3.6 %copy-start.12 = (f32[128]{0:T(128)S(1)}, f32[128]{0:T(128)}, u32[]{:S(2)}) copy-start(f32[128]{0:T(128)} %param.22) | copy-start | bytes 1540
  163.4 3.8 %copy-start.7 = (f32[512,32]{0,1:T(8,128)S(1)}, f32[512,32]{0,1:T(8,128)}, u32[]{:S(2)}) copy-start(f32[512,32]{0,1:T(8,128)} %copy-done.6) | copy-start | bytes 196612
  163.4 3.8 %copy-start.9 = (f32[512,32]{0,1:T(8,128)S(1)}, f32[512,32]{0,1:T(8,128)}, u32[]{:S(2)}) copy-start(f32[512,32]{0,1:T(8,128)} %copy-done.8) | copy-start | bytes 196612
  175.3 0.8 copy-start.1
  176.1 1.6 copy-start.5
  243.6 33.8 %copy-start.2 = (bf16[128,2048]{1,0:T(8,128)(2,1)S(1)}, bf16[128,2048]{1,0:T(8,128)(2,1)}, u32[]{:S(2)}) copy-start(bf16[128,2048]{1,0:T(8,128)(2,1)} %param.13) | copy-start | bytes 1572868
  243.6 33.8 %copy-start.10 = (f32[1,2048]{1,0:T(1,128)S(1)}, f32[1,2048]{1,0:T(1,128)}, u32[]{:S(2)}) copy-start(f32[1,2048]{1,0:T(1,128)} %get-tuple-element.103) | copy-start | bytes 24580
Sparse Core Ops, SparseCore 0:
  57.1 19.8 all-gather.3
  86.6 52.3 all-gather.5
  141.2 47.7 all-gather.7
  246.4 29.7 reduce-scatter.1
where the time goes:
time: 287 us; the launch traced here: 286 us
  blocking collectives  109 us (38%)
  waiting for transfers between devices  57.5 us (20%)
  matrix products  55.5 us (19%)
  other arithmetic  36.5 us (13%)
  local copies, waits for them, and re-layouts  13.9 us (5%)
  between operations  13.4 us (5%)
    psum x1, blocking collectives, body(): summed = lax.psum(partials, 'sp')  38.8 us
    all_gather x1, blocking collectives, body(): lax.all_gather(local_values, 'sp', axis=0, tiled=True)  33.5 us
    all_gather x1, blocking collectives, body(): lax.all_gather(local_keys, 'sp', axis=0, tiled=True)  31.6 us
    reduce_scatter x1, waiting for transfers between devices, body(): lax.psum_scatter(jnp.dot(attended, out_weight, preferred_element_type=jnp...  29.9 us
    dot_general x2, matrix products, update(): jnp.einsum('hqd,khd->hqk', grouped, key_block, preferred_element_type=jnp...  18.8 us
    all_gather x1, waiting for transfers between devices, body(): piece = lax.all_gather(normalised_rows, 'tp', axis=0, tiled=True)  17.4 us
    reduce_sum x2, other arithmetic, update(): jnp.sum(weights_now, axis=-1)  17 us
    dot_general x2, matrix products, update(): jnp.einsum('hqk,khd->hqd', weights_now.astype(jnp.bfloat16), value_block,...  16.2 us
  transfers between devices with their start and end apart: 4, of which 3 were waited for; matrix products, arithmetic and copies ran while one was open for 10% of the time, Pallas kernels for 0%

commit v1 on v0

--- a/solution.py
+++ b/solution.py
@@ -66,7 +66,11 @@
     partials = jnp.dot(
         jax.nn.silu(jnp.stack([cond, ctx_cond])), mod_weight, precision=lax.Precision.HIGHEST
     )
-    summed = lax.psum(partials, "sp")
+    peers = lax.axis_size("sp")
+    summed, far = (partials, 1)
+    while far < peers:
+        summed = summed + lax.ppermute(summed, "sp", [(i, i ^ far) for i in range(peers)])
+        far = 2 * far
     modulation = lax.all_gather(summed, "tp", axis=1, tiled=True)
     gate_vec = modulation[0, 2 * model_width :]
     normalised_rows = modulate(latents, modulation[0])

time: 287 us -> 265 us (0.923)
  blocking collectives: 109 us -> 70.7 us
  starting transfers between devices: 0.13 us -> 8.38 us
  waiting for transfers between devices: 57.5 us -> 64.8 us
    psum x1 -> x0, blocking collectives: 38.8 us -> none  [body(): summed = lax.psum(partials, 'sp')]
    ppermute x0 -> x3, starting transfers between devices: none -> 8.25 us  [body(): lax.ppermute(summed, 'sp', [(i, i ^ far) for i in range(peers)])]
    all_gather x1, waiting for transfers between devices: 17.4 us -> 21.7 us  [body(): piece = lax.all_gather(normalised_rows, 'tp', axis=0, tiled=True)]
    ppermute x0 -> x3, waiting for transfers between devices: none -> 3.79 us  [body(): lax.ppermute(summed, 'sp', [(i, i ^ far) for i in range(peers)])]
  transfers between devices with their start and end apart: 4 -> 7, of which waited for: 3 -> 6; matrix products, arithmetic and copies ran while one was open for 10% -> 12% of each run, Pallas kernels for 0% -> 0%
where the time goes in v1:
time: 265 us; the launch traced here: 264 us
  blocking collectives  70.7 us (27%)
  waiting for transfers between devices  64.8 us (24%)
  matrix products  56.1 us (21%)
  other arithmetic  37 us (14%)
  between operations  13.4 us (5%)
  local copies, waits for them, and re-layouts  13.3 us (5%)
  starting transfers between devices  8.38 us (3%)
    all_gather x1, blocking collectives, body(): lax.all_gather(local_values, 'sp', axis=0, tiled=True)  33.7 us
    all_gather x1, blocking collectives, body(): lax.all_gather(local_keys, 'sp', axis=0, tiled=True)  31.9 us
    reduce_scatter x1, waiting for transfers between devices, body(): lax.psum_scatter(jnp.dot(attended, out_weight, preferred_element_type=jnp...  29.8 us
    all_gather x1, waiting for transfers between devices, body(): piece = lax.all_gather(normalised_rows, 'tp', axis=0, tiled=True)  21.7 us
    dot_general x2, matrix products, update(): jnp.einsum('hqd,khd->hqk', grouped, key_block, preferred_element_type=jnp...  18.8 us
    reduce_sum x2, other arithmetic, update(): jnp.sum(weights_now, axis=-1)  17 us
    dot_general x2, matrix products, update(): jnp.einsum('hqk,khd->hqd', weights_now.astype(jnp.bfloat16), value_block,...  16.2 us
    all_gather x1, waiting for transfers between devices, body(): value_piece = lax.all_gather(value_heads, 'sp', axis=0, tiled=True)  9.34 us
  transfers between devices with their start and end apart: 7, of which 6 were waited for; matrix products, arithmetic and copies ran while one was open for 12% of the time, Pallas kernels for 0%

profile of v1, /device:TPU:0, one launch (start us, length us, event | category | flops | bytes accessed | tf_op | source)
XLA Modules:
  0.0 263.9 jit_solution(15910089554831076522)
XLA Ops:
  6.5 2.4 fusion.41
  9.0 3.0 %collective-permute-start = (f32[2,1536]{1,0:T(2,128)S(1)}, f32[2,1536]{1,0:T(2,128)S(1)}, u32[]{:S(2)}, u32[]{:S(2)}) collective-permute-start(f32[2,1536]{1,0:T(2,128)S(1)} %fusion.41), channel_id=1, source_target_pairs={{0,4},{4,0},{8,12},{12,8},{16,20},{20,16},{24,28},{28,24},{1,5},{5... | collective-permute-start | bytes 36872 | tf_op jit(solution)/shard_map/ppermute | solution.py:72
  13.7 2.2 collective-permute-start.1
  17.5 3.1 %collective-permute-start.2 = (f32[2,1536]{1,0:T(2,128)S(1)}, f32[2,1536]{1,0:T(2,128)S(1)}, u32[]{:S(2)}, u32[]{:S(2)}) collective-permute-start(f32[2,1536]{1,0:T(2,128)S(1)} %add.165), channel_id=1, source_target_pairs={{0,16},{4,20},{8,24},{12,28},{16,0},{20,4},{24,8},{28,12},{1,17},{... | collective-permute-start | bytes 36872 | tf_op jit(solution)/shard_map/ppermute | solution.py:72
  22.3 5.2 %all_gather.18 = f32[2,6144]{1,0:T(2,128)S(1)} all-gather(f32[2,1536]{1,0:T(2,128)S(1)} %add.166), channel_id=1, replica_groups=mesh['sp'=8,'tp'=4] {'tp'}, dimensions={1}, use_global_device_ids=true | all-gather | bytes 61440 | tf_op jit(solution)/shard_map/all_gather | solution.py:74
  28.1 2.1 fusion.30
  32.8 21.7 %all-gather.4.cloned.1.call-done = bf16[512,2048]{1,0:T(8,128)(2,1)} async-done(((bf16[128,2048]{1,0:T(8,128)(2,1)}), bf16[512,2048]{1,0:T(8,128)(2,1)}) %all-gather.4.cloned.1.call-update) | async-done | bytes 2097168 | tf_op jit(solution)/shard_map/all_gather | solution.py:80
  54.6 4.0 %multiply_reduce_fusion.1 = (f32[512,2]{0,1:T(2,128)}, f32[512,256]{0,1:T(8,128)}) fusion(bf16[512,2048]{1,0:T(8,128)(2,1)} %all-gather.4.cloned.1.call-done, bf16[2048,256]{1,0:T(8,128)(2,1)} %param.19), kind=kOutput, calls=%fused_computation.57 | convolution fusion | flops 537132032 | bytes 3674112 | tf_op jit(solution)/shard_map/dot_general | solution.py:84
  64.8 3.3 %convolution_convert_fusion.1 = bf16[512,256]{0,1:T(8,128)(2,1)} fusion(bf16[512,2048]{1,0:T(8,128)(2,1)} %all-gather.4.cloned.1.call-done, bf16[2048,256]{1,0:T(8,128)(2,1)} %param.20), kind=kOutput, calls=%fused_computation.32 | convolution fusion | flops 537001984 | bytes 3407872 | tf_op jit(solution)/shard_map/dot_general | solution.py:85
  76.5 31.9 %all_gather.20 = bf16[512,2,128]{2,0,1:T(8,128)(2,1)S(1)} all-gather(bf16[64,2,128]{2,0,1:T(8,128)(2,1)S(1)} %fusion.37), channel_id=1, replica_groups=mesh['sp'=8,'tp'=4] {'sp'}, dimensions={0}, use_global_device_ids=true | all-gather | bytes 294912 | tf_op jit(solution)/shard_map/all_gather | solution.py:107
  108.4 33.7 %all_gather.21 = bf16[512,2,128]{2,0,1:T(8,128)(2,1)} all-gather(bf16[64,2,128]{2,0,1:T(8,128)(2,1)S(1)} %bitcast.103), channel_id=1, replica_groups=mesh['sp'=8,'tp'=4] {'sp'}, dimensions={0}, use_global_device_ids=true | all-gather | bytes 294912 | tf_op jit(solution)/shard_map/all_gather | solution.py:108
  142.1 3.6 %multiply_reduce_fusion = (f32[512,4]{0,1:T(4,128)S(1)}, f32[512,512]{0,1:T(8,128)S(1)}) fusion(bf16[512,2048]{1,0:T(8,128)(2,1)} %all-gather.4.cloned.1.call-done, bf16[2048,512]{1,0:T(8,128)(2,1)} %param.18), kind=kOutput, calls=%fused_computation.44 | convolution fusion | flops 1074264064 | bytes 5251072 | tf_op jit(solution)/shard_map/dot_general | solution.py:83
  150.1 1.9 copy.75
  157.6 9.3 %all-gather.8.cloned.1.call-done = bf16[4096,2,128]{2,0,1:T(8,128)(2,1)} async-done(((bf16[512,2,128]{2,0,1:T(8,128)(2,1)}), bf16[4096,2,128]{2,0,1:T(8,128)(2,1)}) %all-gather.8.cloned.1.call-update) | async-done | bytes 2097168 | tf_op jit(solution)/shard_map/all_gather | solution.py:152
  166.9 52.2 %while.14 = (s32[]{:T(128)}, f32[2,1024]{1,0:T(2,128)S(1)}, f32[2,1024]{1,0:T(2,128)S(1)}, f32[2,1024,128]{2,1,0:T(8,128)S(1)}, bf16[2,2048,2,128]{3,1,0,2:T(8,1...) while((s32[]{:T(128)}, f32[2,1024]{1,0:T(2,128)S(1)}, ...), condition=%wide.region_10.11_spmd, body=%wide.region_7.10_spmd.sunk | while | flops 2181566464 | bytes 55182420 | solution.py:162
  166.9 9.4 %bitcast_reduce_fusion.2 = (f32[2,1024]{1,0:T(2,128)S(1)}, f32[2,2048,1024]{2,1,0:T(8,128)}) fusion(bf16[2,1024,128]{2,1,0:T(8,128)(2,1)} %get-tuple-element.194, bf16[2,2048,2,128]{3,1,0,2:T(8,128)(2,1)} %get-tuple-element.193, s32[]{:T(128)} %get-tuple-element.181), kind=kOutput, calls=%fused_computation.1.clone.1 | convolution fusion | flops 1082128384 | bytes 18358784 | tf_op jit(solution)/shard_map/while/body/eval_jaxpr/hqd,khd->hqk/dot_general | solution.py:137
  176.3 8.5 %fusion.80 = f32[2,1024]{1,0:T(2,128)S(1)} fusion(f32[2,2048,1024]{2,1,0:T(8,128)} %get-tuple-element.170, f32[2,1024]{1,0:T(2,128)S(1)} %max.4), kind=kLoop, calls=%fused_computation.4.clone.1 | loop fusion | flops 12580864 | bytes 16793600 | tf_op jit(solution)/shard_map/while/body/eval_jaxpr/reduce_sum | solution.py:149
  184.8 8.1 %fusion.81 = f32[2,1024,128]{2,1,0:T(8,128)S(1)} fusion(f32[2,2048,1024]{2,1,0:T(8,128)} %get-tuple-element.170, f32[2,1024]{1,0:T(2,128)S(1)} %max.4, bf16[2,2048,2,128]{3,1,0,2:T(8,128)(2,1)} %get-tuple-element.195, s32[]{:T(128)} %get-tuple-element.181, f32[2,1024,128]{2,1,0:T(8,128)S(1)} %get-tuple-element.184, f32[2,1024]{1,0:T(2,128)S(1)} %get-tuple-element.172), kind=kOutput, calls=%fused_computation.6.clone.1 | convolution fusion | flops 1086849024 | bytes 19939840 | tf_op jit(solution)/shard_map/while/body/eval_jaxpr/hqk,khd->hqd/dot_general | solution.py:143
  193.0 9.4 %bitcast_reduce_fusion.2 = (f32[2,1024]{1,0:T(2,128)S(1)}, f32[2,2048,1024]{2,1,0:T(8,128)}) fusion(bf16[2,1024,128]{2,1,0:T(8,128)(2,1)} %get-tuple-element.194, bf16[2,2048,2,128]{3,1,0,2:T(8,128)(2,1)} %get-tuple-element.193, s32[]{:T(128)} %get-tuple-element.181), kind=kOutput, calls=%fused_computation.1.clone.1 | convolution fusion | flops 1082128384 | bytes 18358784 | tf_op jit(solution)/shard_map/while/body/eval_jaxpr/hqd,khd->hqk/dot_general | solution.py:137
  202.4 8.5 %fusion.80 = f32[2,1024]{1,0:T(2,128)S(1)} fusion(f32[2,2048,1024]{2,1,0:T(8,128)} %get-tuple-element.170, f32[2,1024]{1,0:T(2,128)S(1)} %max.4), kind=kLoop, calls=%fused_computation.4.clone.1 | loop fusion | flops 12580864 | bytes 16793600 | tf_op jit(solution)/shard_map/while/body/eval_jaxpr/reduce_sum | solution.py:149
  210.9 8.1 %fusion.81 = f32[2,1024,128]{2,1,0:T(8,128)S(1)} fusion(f32[2,2048,1024]{2,1,0:T(8,128)} %get-tuple-element.170, f32[2,1024]{1,0:T(2,128)S(1)} %max.4, bf16[2,2048,2,128]{3,1,0,2:T(8,128)(2,1)} %get-tuple-element.195, s32[]{:T(128)} %get-tuple-element.181, f32[2,1024,128]{2,1,0:T(8,128)S(1)} %get-tuple-element.184, f32[2,1024]{1,0:T(2,128)S(1)} %get-tuple-element.172), kind=kOutput, calls=%fused_computation.6.clone.1 | convolution fusion | flops 1086849024 | bytes 19939840 | tf_op jit(solution)/shard_map/while/body/eval_jaxpr/hqk,khd->hqd/dot_general | solution.py:143
  221.5 2.6 convolution_convert_fusion
  224.1 29.8 %reduce-scatter.2.cloned.1.call-done = bf16[128,2048]{1,0:T(8,128)(2,1)} async-done(((bf16[512,2048]{1,0:T(8,128)(2,1)}), bf16[128,2048]{1,0:T(8,128)(2,1)}) %reduce-scatter.2.cloned.1.call-update) | async-done | bytes 524304 | tf_op jit(solution)/shard_map/reduce_scatter | solution.py:170
  255.2 2.1 fusion.31
  (85 shorter events, 36.4 us)
Async XLA Ops:
  6.5 214.9 %copy-start = (bf16[512,2048]{1,0:T(8,128)(2,1)S(1)}, bf16[512,2048]{1,0:T(8,128)(2,1)}, u32[]{:S(2)}) copy-start(bf16[512,2048]{1,0:T(8,128)(2,1)} %param.21) | copy-start | bytes 6291460
  6.5 48.0 %all-gather.4.cloned.1.call-start = ((), (), s32[]{:S(2)}) async-start(), calls=%async_computation.1 | async-start | bytes 2621440 | tf_op jit(solution)/shard_map/all_gather | solution.py:80
  9.0 4.7 %collective-permute-start = (f32[2,1536]{1,0:T(2,128)S(1)}, f32[2,1536]{1,0:T(2,128)S(1)}, u32[]{:S(2)}, u32[]{:S(2)}) collective-permute-start(f32[2,1536]{1,0:T(2,128)S(1)} %fusion.41), channel_id=1, source_target_pairs={{0,4},{4,0},{8,12},{12,8},{16,20},{20,16},{24,28},{28,24},{1,5},{5... | collective-permute-start | bytes 36872 | tf_op jit(solution)/shard_map/ppermute | solution.py:72
  13.7 3.8 %collective-permute-start.1 = (f32[2,1536]{1,0:T(2,128)S(1)}, f32[2,1536]{1,0:T(2,128)S(1)}, u32[]{:S(2)}, u32[]{:S(2)}) collective-permute-start(f32[2,1536]{1,0:T(2,128)S(1)} %add.164), channel_id=1, source_target_pairs={{0,8},{4,12},{8,0},{12,4},{16,24},{20,28},{24,16},{28,20},{1,9},{5... | collective-permute-start | bytes 36872 | tf_op jit(solution)/shard_map/ppermute | solution.py:72
  17.5 4.8 %collective-permute-start.2 = (f32[2,1536]{1,0:T(2,128)S(1)}, f32[2,1536]{1,0:T(2,128)S(1)}, u32[]{:S(2)}, u32[]{:S(2)}) collective-permute-start(f32[2,1536]{1,0:T(2,128)S(1)} %add.165), channel_id=1, source_target_pairs={{0,16},{4,20},{8,24},{12,28},{16,0},{20,4},{24,8},{28,12},{1,17},{... | collective-permute-start | bytes 36872 | tf_op jit(solution)/shard_map/ppermute | solution.py:72
  30.2 127.3 %all-gather.6.cloned.1.call-start = ((), (), s32[]{:S(2)}) async-start(), calls=%async_computation.2 | async-start | bytes 2359296 | tf_op jit(solution)/shard_map/all_gather | solution.py:151
  30.8 23.7 %copy-start.6 = (f32[512,32]{0,1:T(8,128)}, f32[512,32]{0,1:T(8,128)S(1)}, u32[]{:S(2)}) copy-start(f32[512,32]{0,1:T(8,128)S(1)} %get-tuple-element.112) | copy-start | bytes 196612
  30.9 23.7 %copy-start.8 = (f32[512,32]{0,1:T(8,128)}, f32[512,32]{0,1:T(8,128)S(1)}, u32[]{:S(2)}) copy-start(f32[512,32]{0,1:T(8,128)S(1)} %get-tuple-element.113) | copy-start | bytes 196612
  58.6 5.5 %copy-start.3 = (bf16[64,2048]{1,0:T(8,128)(2,1)S(1)}, bf16[64,2048]{1,0:T(8,128)(2,1)}, u32[]{:S(2)}) copy-start(bf16[64,2048]{1,0:T(8,128)(2,1)} %param.14) | copy-start | bytes 786436
  62.9 8.3 %copy-start.4 = (bf16[2048,256]{1,0:T(8,128)(2,1)S(1)}, bf16[2048,256]{1,0:T(8,128)(2,1)}, u32[]{:S(2)}) copy-start(bf16[2048,256]{1,0:T(8,128)(2,1)} %param.19) | copy-start | bytes 3145732
  64.0 102.9 %all-gather.8.cloned.1.call-start = ((), (), s32[]{:S(2)}) async-start(), calls=%async_computation.3 | async-start | bytes 2359296 | tf_op jit(solution)/shard_map/all_gather | solution.py:152
  69.9 184.0 %reduce-scatter.2.cloned.1.call-start = ((), (), s32[]{:S(2)}) async-start(), calls=%async_computation.4 | async-start | bytes 2621440 | tf_op jit(solution)/shard_map/reduce_scatter | solution.py:170
  142.0 3.6 %copy-start.11 = (f32[128]{0:T(128)S(1)}, f32[128]{0:T(128)}, u32[]{:S(2)}) copy-start(f32[128]{0:T(128)} %param.22) | copy-start | bytes 1540
  142.0 3.8 %copy-start.7 = (f32[512,32]{0,1:T(8,128)S(1)}, f32[512,32]{0,1:T(8,128)}, u32[]{:S(2)}) copy-start(f32[512,32]{0,1:T(8,128)} %copy-done.6) | copy-start | bytes 196612
  142.0 3.8 %copy-start.9 = (f32[512,32]{0,1:T(8,128)S(1)}, f32[512,32]{0,1:T(8,128)}, u32[]{:S(2)}) copy-start(f32[512,32]{0,1:T(8,128)} %copy-done.8) | copy-start | bytes 196612
  153.9 0.8 copy-start.1
  154.7 1.6 copy-start.5
  221.5 33.7 %copy-start.2 = (bf16[128,2048]{1,0:T(8,128)(2,1)S(1)}, bf16[128,2048]{1,0:T(8,128)(2,1)}, u32[]{:S(2)}) copy-start(bf16[128,2048]{1,0:T(8,128)(2,1)} %param.13) | copy-start | bytes 1572868
  221.5 33.7 %copy-start.10 = (f32[1,2048]{1,0:T(1,128)S(1)}, f32[1,2048]{1,0:T(1,128)}, u32[]{:S(2)}) copy-start(f32[1,2048]{1,0:T(1,128)} %get-tuple-element.103) | copy-start | bytes 24580
Sparse Core Ops, SparseCore 0:
  30.3 24.1 all-gather.3
  64.1 52.6 all-gather.5
  119.1 47.7 all-gather.7
  224.3 29.6 reduce-scatter.1
